TPU v7x, 32 devices: a whole 2x2x4 slice. The times are simulated.
32 devices in a mesh: kv: 8 (over z, y), tp: 4 (over x, core).
Axes of the slice: x: 2, y: 2, z: 4, core: 2. Of those that a mesh axis runs over, the one named last changes fastest.
Arguments:
- hidden_in: bfloat16 [16, 4096], P(None, ('kv', 'tp')), may hold values from -12 to 12
- attn_gain: float32 [4096], P('kv'), may hold values from 0.1 to 1.9
- query_weight: bfloat16 [4096, 4096], P('kv', 'tp'), may hold values from -0.09375 to 0.09375
- key_cache: bfloat16 [16, 8192, 8, 128], P(None, 'kv', 'tp'), may hold values from -600 to 600
- value_cache: bfloat16 [16, 8192, 8, 128], P(None, 'kv', 'tp'), may hold values from -6 to 6
- lambdas: float32 [32], P('tp'), may hold values from 0.3 to 0.8
- head_gain: float32 [128], replicated, may hold values from 0.1 to 1.9
- out_weight: bfloat16 [4096, 4096], P('tp', 'kv'), may hold values from -0.09375 to 0.09375
- mixer_gain: float32 [4096], P(('kv', 'tp')), may hold values from 0.1 to 1.9
- gate_weight: bfloat16 [4096, 11264], P('kv', 'tp'), may hold values from -0.09375 to 0.09375
- up_weight: bfloat16 [4096, 11264], P('kv', 'tp'), may hold values from -0.09375 to 0.09375
- down_weight: bfloat16 [11264, 4096], P('tp', 'kv'), may hold values from -0.0546875 to 0.0546875
Outputs:
- mixed: bfloat16 [16, 4096], P(None, ('kv', 'tp'))
All inputs are finite; a program needn't handle non-finite values.
Results may differ from a plain program's by a relative error of at most 0.017.
Values may be sent and summed in bfloat16 or wider, within the bound.
A program may use at most 64 MiB of HBM per device.

v0:
```python
import jax
import jax.numpy as jnp
from jax import lax
from jax.sharding import PartitionSpec as P

D = 4096
HEAD_DIM = 64
eps = 1e-06


def finish_heads(totals, weighted, lambdas, head_gain, kv_dev, group_size):
    head_means = weighted / totals[..., None]
    mixing = lambdas.reshape(kv_dev, group_size)
    attended = head_means[0] - mixing[None, :, :, None] * head_means[1]
    norm_inv = lax.rsqrt(jnp.mean(attended * attended, axis=-1, keepdims=True) + eps)
    head_out = (attended * norm_inv * head_gain).astype(jnp.bfloat16)
    return head_out.reshape(head_out.shape[0], kv_dev * group_size * 2 * HEAD_DIM)


def per_device(
    hidden_in,
    attn_gain,
    query_weight,
    key_cache,
    value_cache,
    lambdas,
    head_gain,
    out_weight,
    mixer_gain,
    gate_weight,
    up_weight,
    down_weight,
):
    batch_rows = hidden_in.shape[0]
    rows_block = lax.all_gather(hidden_in, "tp", axis=1, tiled=True)
    block_f = rows_block.astype(jnp.float32)
    gained = (block_f * attn_gain).astype(jnp.bfloat16)
    partial_value = jnp.dot(gained, query_weight, preferred_element_type=jnp.float32)
    own_cols = hidden_in.astype(jnp.float32)
    squares = lax.psum(jnp.sum(own_cols * own_cols, axis=1), ("kv", "tp"))
    query_full = lax.psum(partial_value, "kv")
    row_scale = lax.rsqrt(squares / D + eps)
    query_rows = (query_full * row_scale[:, None]).astype(jnp.bfloat16)
    positions = key_cache.shape[1]
    kv_dev = key_cache.shape[2]
    heads_dev = query_rows.shape[1] // (2 * HEAD_DIM)
    group_size = heads_dev // kv_dev
    query_heads = query_rows.reshape(batch_rows, kv_dev, group_size, 2, HEAD_DIM)
    key_rows = key_cache.reshape(batch_rows, positions, kv_dev, 2, HEAD_DIM)
    scores = jnp.einsum(
        "bkgcd,bpkcd->cbkgp", query_heads, key_rows, preferred_element_type=jnp.float32
    ) * HEAD_DIM ** (-0.5)
    maxima = jnp.max(scores, axis=-1)
    exponent = jnp.exp(scores - maxima[..., None])
    totals = jnp.sum(exponent, axis=-1)
    exp_weights = exponent.astype(jnp.bfloat16)
    weighted = jnp.einsum(
        "cbkgp,bpkv->cbkgv", exp_weights, value_cache, preferred_element_type=jnp.float32
    )
    parts_max, parts_tot, parts_acc = (
        lax.all_to_all(maxima[None], "kv", split_axis=2, concat_axis=0, tiled=True),
        lax.all_to_all(totals[None], "kv", split_axis=2, concat_axis=0, tiled=True),
        lax.all_to_all(weighted[None], "kv", split_axis=2, concat_axis=0, tiled=True),
    )
    top = jnp.max(parts_max, axis=0)
    factors = jnp.exp(parts_max - top[None])
    own_tot = jnp.sum(parts_tot * factors, axis=0)
    own_acc = jnp.sum(parts_acc * factors[..., None], axis=0)
    own_out = finish_heads(own_tot, own_acc, lambdas, head_gain, kv_dev, group_size)
    head_out = lax.all_gather(own_out, "kv", axis=0, tiled=True)
    projected = jnp.dot(head_out, out_weight, preferred_element_type=jnp.float32)
    attn_out = lax.psum_scatter(
        projected.astype(jnp.bfloat16), "tp", scatter_dimension=1, tiled=True
    ).astype(jnp.float32)
    after_attn = (hidden_in.astype(jnp.float32) + attn_out).astype(jnp.bfloat16)
    after_f = after_attn.astype(jnp.float32)
    squares_two = lax.psum(jnp.sum(after_f * after_f, axis=1), ("kv", "tp"))
    mixer_in = (after_f * lax.rsqrt(squares_two / D + eps)[:, None] * mixer_gain).astype(
        jnp.bfloat16
    )
    gathered = lax.all_gather(mixer_in, "tp", axis=1, tiled=True)
    gate_part = jnp.dot(gathered, gate_weight, preferred_element_type=jnp.float32)
    up_part = jnp.dot(gathered, up_weight, preferred_element_type=jnp.float32)
    gate_sum, up_sum = lax.psum((gate_part, up_part), "kv")
    hidden = (jax.nn.silu(gate_sum) * up_sum).astype(jnp.bfloat16)
    down_part = jnp.dot(hidden, down_weight, preferred_element_type=jnp.float32)
    mixer_out = lax.psum_scatter(
        down_part.astype(jnp.bfloat16), "tp", scatter_dimension=1, tiled=True
    ).astype(jnp.float32)
    return (after_f + mixer_out).astype(jnp.bfloat16)


def solution(mesh):
    in_specs = (
        P(None, ("kv", "tp")),
        P("kv"),
        P("kv", "tp"),
        P(None, "kv", "tp", None),
        P(None, "kv", "tp", None),
        P("tp"),
        P(),
        P("tp", "kv"),
        P(("kv", "tp")),
        P("kv", "tp"),
        P("kv", "tp"),
        P("tp", "kv"),
    )
    out_specs = P(None, ("kv", "tp"))
    return jax.shard_map(
        per_device, mesh=mesh, in_specs=in_specs, out_specs=out_specs, check_vma=False
    )
```

profile of v0, /device:TPU:0, one launch (start us, length us, event | category | flops | bytes accessed | tf_op | source)
XLA Modules:
  0.0 329.5 jit_solution(1171620726180046008)
XLA Ops:
  6.5 6.5 %all_gather.9 = bf16[16,512]{1,0:T(8,128)(2,1)S(1)} all-gather(bf16[16,128]{1,0:T(8,128)(2,1)} %param.12), channel_id=1, replica_groups=mesh['kv'=8,'tp'=4] {'tp'}, dimensions={1}, use_global_device_ids=true | all-gather | bytes 20480 | tf_op jit(solution)/shard_map/all_gather | solution.py:35
  13.8 2.1 fusion.15
  16.0 41.0 %psum.36 = f32[16]{0:T(128)S(1)} all-reduce(f32[16]{0:T(128)S(1)} %fusion.17), channel_id=1, replica_groups=mesh['kv'=8,'tp'=4] {'kv','tp'}, use_global_device_ids=true, to_apply=%region_2.0 | all-reduce | flops 16 | bytes 128 | tf_op jit(solution)/shard_map/psum | solution.py:40
  57.0 21.2 %copy.33 = bf16[16,1024,2,128]{1,3,2,0:T(8,128)(2,1)} copy(bf16[16,1024,2,128]{3,2,1,0:T(2,128)(2,1)} %param.15) | data formatting | bytes 16777216 | tf_op args[3]
  78.2 9.0 %all-reduce.4.cloned.1.call-done = f32[16,1024]{1,0:T(8,128)} async-done(((f32[16,1024]{1,0:T(8,128)}), f32[16,1024]{1,0:T(8,128)}) %all-reduce.4.cloned.1.call-update) | async-done | bytes 65552 | tf_op jit(solution)/shard_map/psum | solution.py:41
  87.1 0.9 multiply_convert_fusion.2
  88.2 4.7 %fusion.28 = (f32[2,16,2,4]{3,2,1,0:T(2,128)S(1)}, f32[2,16,2,4,1024]{4,3,2,1,0:T(4,128)S(1)}) fusion(bf16[16,1024,2,2,64]{1,4,3,2,0:T(8,128)(2,1)} %bitcast.56, bf16[16,2,4,2,64]{4,3,2,1,0:T(2,128)(2,1)S(1)} %reshape.35), kind=kOutput, calls=%fused_computation.46 | convolution fusion | flops 34078464 | bytes 9470976 | tf_op jit(solution)/shard_map/bkgcd,bpkcd->cbkgp/dot_general | solution.py:50
  94.1 4.5 %all-to-all-start.2 = ((f32[1,2,16,2,4]{4,3,1,0,2:T(2,128)}), f32[1,2,16,2,4]{4,3,1,0,2:T(2,128)S(1)}, u32[]{:S(2)}, u32[]{:S(2)}) async-start(f32[1,2,16,2,4]{4,3,1,0,2:T(2,128)} %copy.41), calls=%async_computation.2 | async-start | bytes 65536 | tf_op jit(solution)/shard_map/all_to_all | solution.py:62
  99.3 6.1 %all-to-all-done.2 = f32[1,2,16,2,4]{4,3,1,0,2:T(2,128)S(1)} async-done(((f32[1,2,16,2,4]{4,3,1,0,2:T(2,128)}), f32[1,2,16,2,4]{4,3,1,0,2:T(2,128)S(1)}, u32[]{:S(2)}, u32[]{:S(2)}) %all-to-all-start.2) | async-done | bytes 1056 | tf_op jit(solution)/shard_map/all_to_all | solution.py:62
  105.3 3.3 %all-to-all-start.1 = ((f32[1,2,16,2,4]{4,3,1,0,2:T(2,128)}), f32[1,2,16,2,4]{4,3,1,0,2:T(2,128)S(1)}, u32[]{:S(2)}, u32[]{:S(2)}) async-start(f32[1,2,16,2,4]{4,3,1,0,2:T(2,128)} %copy.39), calls=%async_computation.1 | async-start | bytes 65536 | tf_op jit(solution)/shard_map/all_to_all | solution.py:61
  108.7 5.5 %fusion.7 = f32[1,2,16,2,4,128]{5,4,1,3,0,2:T(4,128)} fusion(bf16[16,1024,2,128,1]{3,2,1,0,4:T(2,128)(2,1)} %bitcast.69, bf16[2,16,2,4,1024]{4,3,2,1,0:T(4,128)(2,1)S(1)} %get-tuple-element.10), kind=kOutput, calls=%fused_computation.5 | convolution fusion | flops 67108864 | bytes 9043968 | tf_op jit(solution)/shard_map/cbkgp,bpkv->cbkgv/dot_general | solution.py:57
  114.2 1.1 all-to-all-done.1
  115.3 4.8 %all-to-all-start = ((f32[1,2,16,2,4,128]{5,4,1,3,0,2:T(4,128)}), f32[1,2,16,2,4,128]{5,4,1,3,0,2:T(4,128)S(1)}, u32[]{:S(2)}, u32[]{:S(2)}) async-start(f32[1,2,16,2,4,128]{5,4,1,3,0,2:T(4,128)} %fusion.7), calls=%async_computation | async-start | bytes 262144 | tf_op jit(solution)/shard_map/all_to_all | solution.py:63
  120.4 7.1 %all-to-all-done = f32[1,2,16,2,4,128]{5,4,1,3,0,2:T(4,128)S(1)} async-done(((f32[1,2,16,2,4,128]{5,4,1,3,0,2:T(4,128)}), f32[1,2,16,2,4,128]{5,4,1,3,0,2:T(4,128)S(1)}, u32[]{:S(2)}, u32[]{:S(2)}) %all-to-all-start) | async-done | bytes 131104 | tf_op jit(solution)/shard_map/all_to_all | solution.py:63
  128.1 30.6 %all-gather = bf16[8,2,1024]{2,1,0:T(2,128)(2,1)S(1)} all-gather(bf16[1,2,1024]{2,1,0:T(2,128)(2,1)S(1)} %fusion.25), channel_id=1, replica_groups=mesh['kv'=8,'tp'=4] {'kv'}, dimensions={0}, use_global_device_ids=true | all-gather | bytes 36864 | tf_op jit(solution)/shard_map/all_gather | solution.py:70
  158.8 1.5 convolution_convert_fusion.1
  161.1 17.5 %reduce-scatter.7.cloned.1.call-done = bf16[128,16]{1,0:T(8,128)(2,1)} async-done(((bf16[512,16]{1,0:T(8,128)(2,1)}), bf16[128,16]{1,0:T(8,128)(2,1)}) %reduce-scatter.7.cloned.1.call-update) | async-done | bytes 4112
  179.5 39.3 %psum.37 = f32[16]{0:T(128)S(1)} all-reduce(f32[16]{0:T(128)S(1)} %fusion.19), channel_id=1, replica_groups=mesh['kv'=8,'tp'=4] {'kv','tp'}, use_global_device_ids=true, to_apply=%region_11.0 | all-reduce | flops 16 | bytes 128 | tf_op jit(solution)/shard_map/psum | solution.py:77
  218.9 5.6 %all_gather.11 = bf16[16,512]{1,0:T(8,128)(2,1)S(1)} all-gather(bf16[16,128]{1,0:T(8,128)(2,1)S(1)} %fusion.21), channel_id=1, replica_groups=mesh['kv'=8,'tp'=4] {'tp'}, dimensions={1}, use_global_device_ids=true | all-gather | bytes 20480 | tf_op jit(solution)/shard_map/all_gather | solution.py:81
  224.5 1.2 fusion.29
  225.6 1.2 fusion.30
  226.9 72.3 %all-reduce.6.cloned.1.call-done = (f32[16,2816]{1,0:T(8,128)}, f32[16,2816]{1,0:T(8,128)}) async-done(((f32[16,2816]{1,0:T(8,128)}, f32[16,2816]{1,0:T(8,128)}), (f32[16,2816]{1,0:T(8,128)}, f32[16,2816]{1,0:T(8,128)})) %all-reduce.6.cloned.1.call-update) | async-done | bytes 360464 | tf_op jit(solution)/shard_map/psum | solution.py:84
  299.2 2.5 convolution_convert_fusion
  302.5 19.1 %reduce-scatter.9.cloned.1.call-done = bf16[128,16]{1,0:T(8,128)(2,1)} async-done(((bf16[512,16]{1,0:T(8,128)(2,1)}), bf16[128,16]{1,0:T(8,128)(2,1)}) %reduce-scatter.9.cloned.1.call-update) | async-done | bytes 4112
  (52 shorter events, 7.8 us)
Async XLA Ops:
  6.5 217.9 %copy-start = (bf16[512,2816]{1,0:T(8,128)(2,1)S(1)}, bf16[512,2816]{1,0:T(8,128)(2,1)}, u32[]{:S(2)}) copy-start(bf16[512,2816]{1,0:T(8,128)(2,1)} %param.21) | copy-start | bytes 8650756
  6.5 80.6 %all-reduce.4.cloned.1.call-start = ((), (), s32[]{:S(2)}) async-start(), calls=%async_computation.5 | async-start | bytes 131072 | tf_op jit(solution)/shard_map/psum | solution.py:41
  94.1 11.2 %all-to-all-start.2 = ((f32[1,2,16,2,4]{4,3,1,0,2:T(2,128)}), f32[1,2,16,2,4]{4,3,1,0,2:T(2,128)S(1)}, u32[]{:S(2)}, u32[]{:S(2)}) async-start(f32[1,2,16,2,4]{4,3,1,0,2:T(2,128)} %copy.41), calls=%async_computation.2 | async-start | bytes 65536 | tf_op jit(solution)/shard_map/all_to_all | solution.py:62
  105.3 10.0 %all-to-all-start.1 = ((f32[1,2,16,2,4]{4,3,1,0,2:T(2,128)}), f32[1,2,16,2,4]{4,3,1,0,2:T(2,128)S(1)}, u32[]{:S(2)}, u32[]{:S(2)}) async-start(f32[1,2,16,2,4]{4,3,1,0,2:T(2,128)} %copy.39), calls=%async_computation.1 | async-start | bytes 65536 | tf_op jit(solution)/shard_map/all_to_all | solution.py:61
  108.7 11.5 %copy-start.5 = (f32[8]{0:T(128)S(1)}, f32[8]{0:T(128)}, u32[]{:S(2)}) copy-start(f32[8]{0:T(128)} %param.17) | copy-start | bytes 100
  108.7 19.4 %copy-start.3 = (f32[128]{0:T(128)S(1)}, f32[128]{0:T(128)}, u32[]{:S(2)}) copy-start(f32[128]{0:T(128)} %param.18) | copy-start | bytes 1540
  108.7 70.7 %copy-start.2 = (bf16[16,128]{1,0:T(8,128)(2,1)S(1)}, bf16[16,128]{1,0:T(8,128)(2,1)}, u32[]{:S(2)}) copy-start(bf16[16,128]{1,0:T(8,128)(2,1)} %param.12) | copy-start | bytes 12292
  108.7 110.1 %copy-start.4 = (f32[128]{0:T(128)S(1)}, f32[128]{0:T(128)}, u32[]{:S(2)}) copy-start(f32[128]{0:T(128)} %param.20) | copy-start | bytes 1540
  115.3 12.2 %all-to-all-start = ((f32[1,2,16,2,4,128]{5,4,1,3,0,2:T(4,128)}), f32[1,2,16,2,4,128]{5,4,1,3,0,2:T(4,128)S(1)}, u32[]{:S(2)}, u32[]{:S(2)}) async-start(f32[1,2,16,2,4,128]{5,4,1,3,0,2:T(4,128)} %fusion.7), calls=%async_computation | async-start | bytes 262144 | tf_op jit(solution)/shard_map/all_to_all | solution.py:63
  120.1 58.4 %reduce-scatter.7.cloned.1.call-start = ((), (), s32[]{:S(2)}) async-start(), calls=%async_computation.6 | async-start | bytes 163840
  161.0 138.2 %all-reduce.6.cloned.1.call-start = ((), (), s32[]{:S(2)}) async-start(), calls=%async_computation.8 | async-start | bytes 720896 | tf_op jit(solution)/shard_map/psum | solution.py:84
  218.8 6.8 %copy-start.1 = (bf16[512,2816]{1,0:T(8,128)(2,1)S(1)}, bf16[512,2816]{1,0:T(8,128)(2,1)}, u32[]{:S(2)}) copy-start(bf16[512,2816]{1,0:T(8,128)(2,1)} %param.22) | copy-start | bytes 8650756
  226.8 94.8 %reduce-scatter.9.cloned.1.call-start = ((), (), s32[]{:S(2)}) async-start(), calls=%async_computation.7 | async-start | bytes 163840
Sparse Core Ops, SparseCore 0:
  16.1 71.0 all-reduce.3
  161.1 17.3 reduce-scatter.6
  226.9 72.2 all-reduce.5
  302.6 18.9 reduce-scatter.8
where the time goes:
time: 331 us; the launch traced here: 330 us
  waiting for transfers between devices  132 us (40%)
  blocking collectives  123 us (37%)
  local copies, waits for them, and re-layouts  26 us (8%)
  matrix products  18.6 us (6%)
  between operations  13.3 us (4%)
  starting transfers between devices  12.8 us (4%)
  other arithmetic  3.66 us (1%)
    psum x1, waiting for transfers between devices, per_device(): gate_sum, up_sum = lax.psum((gate_part, up_part), 'kv')  72.3 us
    psum x1, blocking collectives, per_device(): squares = lax.psum(jnp.sum(own_cols * own_cols, axis=1), ('kv', 'tp'))  41 us
    psum x1, blocking collectives, per_device(): squares_two = lax.psum(jnp.sum(after_f * after_f, axis=1), ('kv', 'tp'))  39.3 us
    unnamed x6, waiting for transfers between devices  36.7 us
    all_gather x1, blocking collectives, per_device(): head_out = lax.all_gather(own_out, 'kv', axis=0, tiled=True)  30.6 us
    unnamed x18, local copies, waits for them, and re-layouts  24.3 us
    psum x1, waiting for transfers between devices, per_device(): query_full = lax.psum(partial_value, 'kv')  8.99 us
    all_to_all x1, waiting for transfers between devices, per_device(): lax.all_to_all(weighted[None], 'kv', split_axis=2, concat_axis=0, tiled=T...  7.09 us
  transfers between devices with their start and end apart: 7, of which 7 were waited for; matrix products, arithmetic and copies ran while one was open for 8% of the time, Pallas kernels for 0%

commit v1 on v0

--- a/solution.py
+++ b/solution.py
@@ -67,7 +67,12 @@
     own_tot = jnp.sum(parts_tot * factors, axis=0)
     own_acc = jnp.sum(parts_acc * factors[..., None], axis=0)
     own_out = finish_heads(own_tot, own_acc, lambdas, head_gain, kv_dev, group_size)
-    head_out = lax.all_gather(own_out, "kv", axis=0, tiled=True)
+    ring = [own_out]
+    for hop in range(7):
+        ring.append(lax.ppermute(ring[-1], "kv", [(dev, (dev + 1) % 8) for dev in range(8)]))
+    head_out = jnp.roll(
+        jnp.concatenate(ring[::-1], axis=0), (lax.axis_index("kv") + 1) * ring[0].shape[0], axis=0
+    )
     projected = jnp.dot(head_out, out_weight, preferred_element_type=jnp.float32)
     attn_out = lax.psum_scatter(
         projected.astype(jnp.bfloat16), "tp", scatter_dimension=1, tiled=True

time: 331 us -> 344 us (1.039)
  waiting for transfers between devices: 132 us -> 176 us
  blocking collectives: 123 us -> 92.4 us
    ppermute x0 -> x7, waiting for transfers between devices: none -> 43.9 us  [per_device(): lax.ppermute(ring[-1], 'kv', [(dev, (dev + 1) % 8) for dev in range(8)])]
    all_gather x1 -> x0, blocking collectives: 30.6 us -> none  [per_device(): head_out = lax.all_gather(own_out, 'kv', axis=0, tiled=True)]
    unnamed x18 -> x17, local copies, waits for them, and re-layouts: 24.3 us -> 24.3 us
  transfers between devices with their start and end apart: 7 -> 14, of which waited for: 7 -> 14; matrix products, arithmetic and copies ran while one was open for 8% -> 8% of each run, Pallas kernels for 0% -> 0%
where the time goes in v1:
time: 344 us; the launch traced here: 343 us
  waiting for transfers between devices  176 us (51%)
  blocking collectives  92.4 us (27%)
  local copies, waits for them, and re-layouts  26.1 us (8%)
  matrix products  18.6 us (5%)
  between operations  13.3 us (4%)
  starting transfers between devices  13.1 us (4%)
  other arithmetic  3.66 us (1%)
    psum x1, waiting for transfers between devices, per_device(): gate_sum, up_sum = lax.psum((gate_part, up_part), 'kv')  72.3 us
    ppermute x7, waiting for transfers between devices, per_device(): lax.ppermute(ring[-1], 'kv', [(dev, (dev + 1) % 8) for dev in range(8)])  43.9 us
    psum x1, blocking collectives, per_device(): squares = lax.psum(jnp.sum(own_cols * own_cols, axis=1), ('kv', 'tp'))  41 us
    psum x1, blocking collectives, per_device(): squares_two = lax.psum(jnp.sum(after_f * after_f, axis=1), ('kv', 'tp'))  39.3 us
    unnamed x6, waiting for transfers between devices  36.1 us
    unnamed x17, local copies, waits for them, and re-layouts  24.3 us
    psum x1, waiting for transfers between devices, per_device(): query_full = lax.psum(partial_value, 'kv')  9.04 us
    all_to_all x1, waiting for transfers between devices, per_device(): lax.all_to_all(weighted[None], 'kv', split_axis=2, concat_axis=0, tiled=T...  7.09 us
  transfers between devices with their start and end apart: 14, of which 14 were waited for; matrix products, arithmetic and copies ran while one was open for 8% of the time, Pallas kernels for 0%

profile of v1, /device:TPU:0, one launch (start us, length us, event | category | flops | bytes accessed | tf_op | source)
XLA Modules:
  0.0 342.7 jit_solution(5809537493440563807)
XLA Ops:
  6.5 6.5 %all_gather.6 = bf16[16,512]{1,0:T(8,128)(2,1)S(1)} all-gather(bf16[16,128]{1,0:T(8,128)(2,1)} %param.12), channel_id=1, replica_groups=mesh['kv'=8,'tp'=4] {'tp'}, dimensions={1}, use_global_device_ids=true | all-gather | bytes 20480 | tf_op jit(solution)/shard_map/all_gather | solution.py:35
  16.0 41.0 %psum.36 = f32[16]{0:T(128)S(1)} all-reduce(f32[16]{0:T(128)S(1)} %fusion.18), channel_id=1, replica_groups=mesh['kv'=8,'tp'=4] {'kv','tp'}, use_global_device_ids=true, to_apply=%region_2.0 | all-reduce | flops 16 | bytes 128 | tf_op jit(solution)/shard_map/psum | solution.py:40
  56.9 21.2 %copy.33 = bf16[16,1024,2,128]{1,3,2,0:T(8,128)(2,1)} copy(bf16[16,1024,2,128]{3,2,1,0:T(2,128)(2,1)} %param.15) | data formatting | bytes 16777216 | tf_op args[3]
  78.1 9.0 %all-reduce.4.cloned.1.call-done = f32[16,1024]{1,0:T(8,128)} async-done(((f32[16,1024]{1,0:T(8,128)}), f32[16,1024]{1,0:T(8,128)}) %all-reduce.4.cloned.1.call-update) | async-done | bytes 65552 | tf_op jit(solution)/shard_map/psum | solution.py:41
  88.2 4.7 %fusion.29 = (f32[2,16,2,4]{3,2,1,0:T(2,128)S(1)}, f32[2,16,2,4,1024]{4,3,2,1,0:T(4,128)S(1)}) fusion(bf16[16,1024,2,2,64]{1,4,3,2,0:T(8,128)(2,1)} %bitcast.53, bf16[16,2,4,2,64]{4,3,2,1,0:T(2,128)(2,1)S(1)} %reshape.35), kind=kOutput, calls=%fused_computation.47 | convolution fusion | flops 34078464 | bytes 9470976 | tf_op jit(solution)/shard_map/bkgcd,bpkcd->cbkgp/dot_general | solution.py:50
  94.1 4.5 %all-to-all-start.2 = ((f32[1,2,16,2,4]{4,3,1,0,2:T(2,128)}), f32[1,2,16,2,4]{4,3,1,0,2:T(2,128)S(1)}, u32[]{:S(2)}, u32[]{:S(2)}) async-start(f32[1,2,16,2,4]{4,3,1,0,2:T(2,128)} %copy.41), calls=%async_computation.2 | async-start | bytes 65536 | tf_op jit(solution)/shard_map/all_to_all | solution.py:62
  99.3 6.1 %all-to-all-done.2 = f32[1,2,16,2,4]{4,3,1,0,2:T(2,128)S(1)} async-done(((f32[1,2,16,2,4]{4,3,1,0,2:T(2,128)}), f32[1,2,16,2,4]{4,3,1,0,2:T(2,128)S(1)}, u32[]{:S(2)}, u32[]{:S(2)}) %all-to-all-start.2) | async-done | bytes 1056 | tf_op jit(solution)/shard_map/all_to_all | solution.py:62
  105.3 3.3 all-to-all-start.1
  108.7 5.5 %fusion.7 = f32[1,2,16,2,4,128]{5,4,1,3,0,2:T(4,128)} fusion(bf16[16,1024,2,128,1]{3,2,1,0,4:T(2,128)(2,1)} %bitcast.66, bf16[2,16,2,4,1024]{4,3,2,1,0:T(4,128)(2,1)S(1)} %get-tuple-element.10), kind=kOutput, calls=%fused_computation.5 | convolution fusion | flops 67108864 | bytes 9043968 | tf_op jit(solution)/shard_map/cbkgp,bpkv->cbkgv/dot_general | solution.py:57
  115.3 4.8 %all-to-all-start = ((f32[1,2,16,2,4,128]{5,4,1,3,0,2:T(4,128)}), f32[1,2,16,2,4,128]{5,4,1,3,0,2:T(4,128)S(1)}, u32[]{:S(2)}, u32[]{:S(2)}) async-start(f32[1,2,16,2,4,128]{5,4,1,3,0,2:T(4,128)} %fusion.7), calls=%async_computation | async-start | bytes 262144 | tf_op jit(solution)/shard_map/all_to_all | solution.py:63
  120.4 7.1 %all-to-all-done = f32[1,2,16,2,4,128]{5,4,1,3,0,2:T(4,128)S(1)} async-done(((f32[1,2,16,2,4,128]{5,4,1,3,0,2:T(4,128)}), f32[1,2,16,2,4,128]{5,4,1,3,0,2:T(4,128)S(1)}, u32[]{:S(2)}, u32[]{:S(2)}) %all-to-all-start) | async-done | bytes 131104 | tf_op jit(solution)/shard_map/all_to_all | solution.py:63
  128.4 6.1 %collective-permute-done = bf16[2,1024]{1,0:T(2,128)(2,1)S(1)} collective-permute-done((bf16[2,1024]{1,0:T(2,128)(2,1)S(1)}, bf16[2,1024]{1,0:T(2,128)(2,1)S(1)}, u32[]{:S(2)}, u32[]{:S(2)}) %collective-permute-start) | collective-permute-done | bytes 4128 | tf_op jit(solution)/shard_map/ppermute | solution.py:72
  134.5 6.3 %collective-permute-done.1 = bf16[2,1024]{1,0:T(2,128)(2,1)S(1)} collective-permute-done((bf16[2,1024]{1,0:T(2,128)(2,1)S(1)}, bf16[2,1024]{1,0:T(2,128)(2,1)S(1)}, u32[]{:S(2)}, u32[]{:S(2)}) %collective-permute-start.1) | collective-permute-done | bytes 4128 | tf_op jit(solution)/shard_map/ppermute | solution.py:72
  140.8 6.3 %collective-permute-done.2 = bf16[2,1024]{1,0:T(2,128)(2,1)S(1)} collective-permute-done((bf16[2,1024]{1,0:T(2,128)(2,1)S(1)}, bf16[2,1024]{1,0:T(2,128)(2,1)S(1)}, u32[]{:S(2)}, u32[]{:S(2)}) %collective-permute-start.2) | collective-permute-done | bytes 4128 | tf_op jit(solution)/shard_map/ppermute | solution.py:72
  147.1 6.3 %collective-permute-done.3 = bf16[2,1024]{1,0:T(2,128)(2,1)S(1)} collective-permute-done((bf16[2,1024]{1,0:T(2,128)(2,1)S(1)}, bf16[2,1024]{1,0:T(2,128)(2,1)S(1)}, u32[]{:S(2)}, u32[]{:S(2)}) %collective-permute-start.3) | collective-permute-done | bytes 4128 | tf_op jit(solution)/shard_map/ppermute | solution.py:72
  153.4 6.3 %collective-permute-done.4 = bf16[2,1024]{1,0:T(2,128)(2,1)S(1)} collective-permute-done((bf16[2,1024]{1,0:T(2,128)(2,1)S(1)}, bf16[2,1024]{1,0:T(2,128)(2,1)S(1)}, u32[]{:S(2)}, u32[]{:S(2)}) %collective-permute-start.4) | collective-permute-done | bytes 4128 | tf_op jit(solution)/shard_map/ppermute | solution.py:72
  159.7 6.3 %collective-permute-done.5 = bf16[2,1024]{1,0:T(2,128)(2,1)S(1)} collective-permute-done((bf16[2,1024]{1,0:T(2,128)(2,1)S(1)}, bf16[2,1024]{1,0:T(2,128)(2,1)S(1)}, u32[]{:S(2)}, u32[]{:S(2)}) %collective-permute-start.5) | collective-permute-done | bytes 4128 | tf_op jit(solution)/shard_map/ppermute | solution.py:72
  166.0 6.3 %collective-permute-done.6 = bf16[2,1024]{1,0:T(2,128)(2,1)S(1)} collective-permute-done((bf16[2,1024]{1,0:T(2,128)(2,1)S(1)}, bf16[2,1024]{1,0:T(2,128)(2,1)S(1)}, u32[]{:S(2)}, u32[]{:S(2)}) %collective-permute-start.6) | collective-permute-done | bytes 4128 | tf_op jit(solution)/shard_map/ppermute | solution.py:72
  174.8 17.0 %reduce-scatter.7.cloned.1.call-done = bf16[128,16]{1,0:T(8,128)(2,1)} async-done(((bf16[512,16]{1,0:T(8,128)(2,1)}), bf16[128,16]{1,0:T(8,128)(2,1)}) %reduce-scatter.7.cloned.1.call-update) | async-done | bytes 4112
  192.7 39.3 %psum.37 = f32[16]{0:T(128)S(1)} all-reduce(f32[16]{0:T(128)S(1)} %fusion.20), channel_id=1, replica_groups=mesh['kv'=8,'tp'=4] {'kv','tp'}, use_global_device_ids=true, to_apply=%region_11.12 | all-reduce | flops 16 | bytes 128 | tf_op jit(solution)/shard_map/psum | solution.py:82
  232.1 5.6 %all_gather.7 = bf16[16,512]{1,0:T(8,128)(2,1)S(1)} all-gather(bf16[16,128]{1,0:T(8,128)(2,1)S(1)} %fusion.22), channel_id=1, replica_groups=mesh['kv'=8,'tp'=4] {'tp'}, dimensions={1}, use_global_device_ids=true | all-gather | bytes 20480 | tf_op jit(solution)/shard_map/all_gather | solution.py:86
  240.1 72.3 %all-reduce.6.cloned.1.call-done = (f32[16,2816]{1,0:T(8,128)}, f32[16,2816]{1,0:T(8,128)}) async-done(((f32[16,2816]{1,0:T(8,128)}, f32[16,2816]{1,0:T(8,128)}), (f32[16,2816]{1,0:T(8,128)}, f32[16,2816]{1,0:T(8,128)})) %all-reduce.6.cloned.1.call-update) | async-done | bytes 360464 | tf_op jit(solution)/shard_map/psum | solution.py:89
  312.4 2.5 convolution_convert_fusion
  315.7 19.1 %reduce-scatter.9.cloned.1.call-done = bf16[128,16]{1,0:T(8,128)(2,1)} async-done(((bf16[512,16]{1,0:T(8,128)(2,1)}), bf16[128,16]{1,0:T(8,128)(2,1)}) %reduce-scatter.9.cloned.1.call-update) | async-done | bytes 4112
  (65 shorter events, 16.1 us)
Async XLA Ops:
  6.5 231.1 %copy-start = (bf16[512,2816]{1,0:T(8,128)(2,1)S(1)}, bf16[512,2816]{1,0:T(8,128)(2,1)}, u32[]{:S(2)}) copy-start(bf16[512,2816]{1,0:T(8,128)(2,1)} %param.21) | copy-start | bytes 8650756
  6.5 80.6 %all-reduce.4.cloned.1.call-start = ((), (), s32[]{:S(2)}) async-start(), calls=%async_computation.5 | async-start | bytes 131072 | tf_op jit(solution)/shard_map/psum | solution.py:41
  94.1 11.2 %all-to-all-start.2 = ((f32[1,2,16,2,4]{4,3,1,0,2:T(2,128)}), f32[1,2,16,2,4]{4,3,1,0,2:T(2,128)S(1)}, u32[]{:S(2)}, u32[]{:S(2)}) async-start(f32[1,2,16,2,4]{4,3,1,0,2:T(2,128)} %copy.41), calls=%async_computation.2 | async-start | bytes 65536 | tf_op jit(solution)/shard_map/all_to_all | solution.py:62
  105.3 10.0 %all-to-all-start.1 = ((f32[1,2,16,2,4]{4,3,1,0,2:T(2,128)}), f32[1,2,16,2,4]{4,3,1,0,2:T(2,128)S(1)}, u32[]{:S(2)}, u32[]{:S(2)}) async-start(f32[1,2,16,2,4]{4,3,1,0,2:T(2,128)} %copy.39), calls=%async_computation.1 | async-start | bytes 65536 | tf_op jit(solution)/shard_map/all_to_all | solution.py:61
  108.7 11.5 %copy-start.5 = (f32[8]{0:T(128)S(1)}, f32[8]{0:T(128)}, u32[]{:S(2)}) copy-start(f32[8]{0:T(128)} %param.17) | copy-start | bytes 100
  108.7 19.4 %copy-start.3 = (f32[128]{0:T(128)S(1)}, f32[128]{0:T(128)}, u32[]{:S(2)}) copy-start(f32[128]{0:T(128)} %param.18) | copy-start | bytes 1540
  108.7 83.9 %copy-start.2 = (bf16[16,128]{1,0:T(8,128)(2,1)S(1)}, bf16[16,128]{1,0:T(8,128)(2,1)}, u32[]{:S(2)}) copy-start(bf16[16,128]{1,0:T(8,128)(2,1)} %param.12) | copy-start | bytes 12292
  108.7 123.3 %copy-start.4 = (f32[128]{0:T(128)S(1)}, f32[128]{0:T(128)}, u32[]{:S(2)}) copy-start(f32[128]{0:T(128)} %param.20) | copy-start | bytes 1540
  115.3 12.2 %all-to-all-start = ((f32[1,2,16,2,4,128]{5,4,1,3,0,2:T(4,128)}), f32[1,2,16,2,4,128]{5,4,1,3,0,2:T(4,128)S(1)}, u32[]{:S(2)}, u32[]{:S(2)}) async-start(f32[1,2,16,2,4,128]{5,4,1,3,0,2:T(4,128)} %fusion.7), calls=%async_computation | async-start | bytes 262144 | tf_op jit(solution)/shard_map/all_to_all | solution.py:63
  120.1 71.6 %reduce-scatter.7.cloned.1.call-start = ((), (), s32[]{:S(2)}) async-start(), calls=%async_computation.6 | async-start | bytes 163840
  128.1 6.4 %collective-permute-start = (bf16[2,1024]{1,0:T(2,128)(2,1)S(1)}, bf16[2,1024]{1,0:T(2,128)(2,1)S(1)}, u32[]{:S(2)}, u32[]{:S(2)}) collective-permute-start(bf16[2,1024]{1,0:T(2,128)(2,1)S(1)} %multiply_convert_fusion.5), channel_id=1, source_target_pairs={{0,4},{4,8},{8,12},{12,16},{16,20},{20,24},{24,28},{28,0},{1,5},{5... | collective-permute-start | bytes 12296 | tf_op jit(solution)/shard_map/ppermute | solution.py:72
  134.5 6.3 %collective-permute-start.1 = (bf16[2,1024]{1,0:T(2,128)(2,1)S(1)}, bf16[2,1024]{1,0:T(2,128)(2,1)S(1)}, u32[]{:S(2)}, u32[]{:S(2)}) collective-permute-start(bf16[2,1024]{1,0:T(2,128)(2,1)S(1)} %collective-permute-done), channel_id=1, source_target_pairs={{0,4},{4,8},{8,12},{12,16},{16,20},{20,24},{24,28},{28,0},{1,5},{5... | collective-permute-start | bytes 12296 | tf_op jit(solution)/shard_map/ppermute | solution.py:72
  140.8 6.3 %collective-permute-start.2 = (bf16[2,1024]{1,0:T(2,128)(2,1)S(1)}, bf16[2,1024]{1,0:T(2,128)(2,1)S(1)}, u32[]{:S(2)}, u32[]{:S(2)}) collective-permute-start(bf16[2,1024]{1,0:T(2,128)(2,1)S(1)} %collective-permute-done.1), channel_id=1, source_target_pairs={{0,4},{4,8},{8,12},{12,16},{16,20},{20,24},{24,28},{28,0},{1,5},{5... | collective-permute-start | bytes 12296 | tf_op jit(solution)/shard_map/ppermute | solution.py:72
  147.1 6.3 %collective-permute-start.3 = (bf16[2,1024]{1,0:T(2,128)(2,1)S(1)}, bf16[2,1024]{1,0:T(2,128)(2,1)S(1)}, u32[]{:S(2)}, u32[]{:S(2)}) collective-permute-start(bf16[2,1024]{1,0:T(2,128)(2,1)S(1)} %collective-permute-done.2), channel_id=1, source_target_pairs={{0,4},{4,8},{8,12},{12,16},{16,20},{20,24},{24,28},{28,0},{1,5},{5... | collective-permute-start | bytes 12296 | tf_op jit(solution)/shard_map/ppermute | solution.py:72
  153.4 6.3 %collective-permute-start.4 = (bf16[2,1024]{1,0:T(2,128)(2,1)S(1)}, bf16[2,1024]{1,0:T(2,128)(2,1)S(1)}, u32[]{:S(2)}, u32[]{:S(2)}) collective-permute-start(bf16[2,1024]{1,0:T(2,128)(2,1)S(1)} %collective-permute-done.3), channel_id=1, source_target_pairs={{0,4},{4,8},{8,12},{12,16},{16,20},{20,24},{24,28},{28,0},{1,5},{5... | collective-permute-start | bytes 12296 | tf_op jit(solution)/shard_map/ppermute | solution.py:72
  159.7 6.3 %collective-permute-start.5 = (bf16[2,1024]{1,0:T(2,128)(2,1)S(1)}, bf16[2,1024]{1,0:T(2,128)(2,1)S(1)}, u32[]{:S(2)}, u32[]{:S(2)}) collective-permute-start(bf16[2,1024]{1,0:T(2,128)(2,1)S(1)} %collective-permute-done.4), channel_id=1, source_target_pairs={{0,4},{4,8},{8,12},{12,16},{16,20},{20,24},{24,28},{28,0},{1,5},{5... | collective-permute-start | bytes 12296 | tf_op jit(solution)/shard_map/ppermute | solution.py:72
  166.0 6.3 %collective-permute-start.6 = (bf16[2,1024]{1,0:T(2,128)(2,1)S(1)}, bf16[2,1024]{1,0:T(2,128)(2,1)S(1)}, u32[]{:S(2)}, u32[]{:S(2)}) collective-permute-start(bf16[2,1024]{1,0:T(2,128)(2,1)S(1)} %collective-permute-done.5), channel_id=1, source_target_pairs={{0,4},{4,8},{8,12},{12,16},{16,20},{20,24},{24,28},{28,0},{1,5},{5... | collective-permute-start | bytes 12296 | tf_op jit(solution)/shard_map/ppermute | solution.py:72
  174.7 137.7 %all-reduce.6.cloned.1.call-start = ((), (), s32[]{:S(2)}) async-start(), calls=%async_computation.8 | async-start | bytes 720896 | tf_op jit(solution)/shard_map/psum | solution.py:89
  232.0 6.8 %copy-start.1 = (bf16[512,2816]{1,0:T(8,128)(2,1)S(1)}, bf16[512,2816]{1,0:T(8,128)(2,1)}, u32[]{:S(2)}) copy-start(bf16[512,2816]{1,0:T(8,128)(2,1)} %param.22) | copy-start | bytes 8650756
  240.0 94.8 %reduce-scatter.9.cloned.1.call-start = ((), (), s32[]{:S(2)}) async-start(), calls=%async_computation.7 | async-start | bytes 163840
Sparse Core Ops, SparseCore 0:
  16.1 71.0 all-reduce.3
  174.8 16.8 reduce-scatter.6
  240.1 72.2 all-reduce.5
  315.8 18.9 reduce-scatter.8
